TPU v7x, 32 devices: a whole 2x2x4 slice. The times are simulated.
32 devices in a mesh: fs: 4 (over y, x), tp: 8 (over z, core).
Axes of the slice: x: 2, y: 2, z: 4, core: 2. Of those that a mesh axis runs over, the one named last changes fastest.
Arguments:
- tokens: bfloat16 [4096, 2048], P(('fs', 'tp')), may hold values from -6 to 6
- up_gate: bfloat16 [4096, 5632], P('fs', 'tp'), may hold values from -8 to 8
- up_val: bfloat16 [4096, 5632], P('fs', 'tp'), may hold values from -6 to 6
- gate_weight: bfloat16 [2048, 5632], P('fs', 'tp'), may hold values from -0.125 to 0.125
- val_weight: bfloat16 [2048, 5632], P('fs', 'tp'), may hold values from -0.125 to 0.125
- gate_taps: bfloat16 [3, 5632], P(None, 'tp'), may hold values from -3 to 3
- val_taps: bfloat16 [3, 5632], P(None, 'tp'), may hold values from -3 to 3
- hidden_grad: bfloat16 [4096, 5632], P('fs', 'tp'), may hold values from -6 to 6
Outputs:
- input_grad: bfloat16 [4096, 2048], P(('fs', 'tp'))
- gate_weight_grad: float32 [2048, 5632], P('fs', 'tp')
- val_weight_grad: float32 [2048, 5632], P('fs', 'tp')
- gate_taps_grad: float32 [3, 5632], P(None, 'tp')
- val_taps_grad: float32 [3, 5632], P(None, 'tp')
- gate_row_norms: float32 [2048], P('fs')
- val_row_norms: float32 [2048], P('fs')
- tap_row_norms: float32 [2, 3], replicated
All inputs are finite; a program needn't handle non-finite values.
Results may differ from a plain program's by a relative error of at most 0.017.
Values may be sent and summed in bfloat16 or wider, within the bound.
A program may use at most 128 MiB of HBM per device.

v0:
```python
import functools

import jax
import jax.numpy as jnp
from jax import lax
from jax.experimental import pallas as pl
from jax.experimental.pallas import tpu as pltpu
from jax.sharding import PartitionSpec as P

SEQ = 1024
CHUNKS = 4


def backs_kernel(group, gate_ref, val_ref, grad_ref, gate_tap_ref, val_tap_ref, back_ref, tap_ref):
    step, rows = gate_ref.shape
    taps = gate_tap_ref.shape[1]
    place = lax.broadcasted_iota(jnp.int32, (group, rows), 1) % SEQ

    def one(index, carry):
        at = pl.ds(pl.multiple_of(index * group, group), group)
        gate_kernel = gate_tap_ref[at, :]
        val_kernel = val_tap_ref[at, :]

        def delayed(field, shift):
            if shift == 0:
                return field
            return jnp.where(place >= shift, pltpu.roll(field, shift, 1), 0.0)

        def advanced(field, shift):
            if shift == 0:
                return field
            return jnp.where(place < SEQ - shift, pltpu.roll(field, rows - shift, 1), 0.0)

        def mixed(fields, kernel):
            total = fields[0] * kernel[:, 0:1]
            for i in range(1, taps):
                total = total + fields[i] * kernel[:, i : i + 1]
            return total

        gate_fields = [
            delayed(gate_ref[at, :].astype(jnp.float32), taps - 1 - i) for i in range(taps)
        ]
        val_fields = [delayed(val_ref[at, :].astype(jnp.float32), taps - 1 - i) for i in range(taps)]
        conv_gate = mixed(gate_fields, gate_kernel)
        conv_val = mixed(val_fields, val_kernel)
        sigmoid = jax.nn.sigmoid(conv_gate)
        scaled = grad_ref[at, :].astype(jnp.float32) * sigmoid
        val_back = scaled * conv_gate
        gate_back = scaled * conv_val * (1.0 + conv_gate * (1.0 - sigmoid))
        back_ref[at, :] = mixed(
            [advanced(gate_back, taps - 1 - i) for i in range(taps)], gate_kernel
        ).astype(jnp.bfloat16)
        back_ref[pl.ds(pl.multiple_of(step + index * group, group), group), :] = mixed(
            [advanced(val_back, taps - 1 - i) for i in range(taps)], val_kernel
        ).astype(jnp.bfloat16)
        for i in range(taps):
            tap_ref[at, i : i + 1] = jnp.sum(gate_fields[i] * gate_back, axis=1, keepdims=True)
            tap_ref[at, taps + i : taps + i + 1] = jnp.sum(
                val_fields[i] * val_back, axis=1, keepdims=True
            )
        return carry

    lax.fori_loop(0, step // group, one, 0)


def chunk_backs(k, step, up_gate, up_val, hidden_grad, gate_taps, val_taps):
    rows = up_gate.shape[1]
    taps = gate_taps.shape[1]
    group = 16 if step % 16 == 0 else 8
    field = pl.BlockSpec((step, rows), lambda i: (k, 0))
    tap = pl.BlockSpec((step, taps), lambda i: (k, 0))
    return pl.pallas_call(
        functools.partial(backs_kernel, group),
        grid=(1,),
        in_specs=[field, field, field, tap, tap],
        out_specs=[
            pl.BlockSpec((2 * step, rows), lambda i: (0, 0)),
            pl.BlockSpec((step, 2 * taps), lambda i: (0, 0)),
        ],
        out_shape=[
            jax.ShapeDtypeStruct((2 * step, rows), jnp.bfloat16),
            jax.ShapeDtypeStruct((step, 2 * taps), jnp.float32),
        ],
        cost_estimate=pl.CostEstimate(
            flops=60 * step * rows, bytes_accessed=10 * step * rows, transcendentals=step * rows
        ),
    )(up_gate, up_val, hidden_grad, gate_taps, val_taps)


def make_local(fs_size, tp_size):
    rows_b = max(d for d in range(1, fs_size + 1) if fs_size % d == 0 and d * d <= fs_size)
    fb = rows_b
    fa = fs_size // fb
    cores = 2 if tp_size % 2 == 0 else 1
    chips = tp_size // cores

    def from_b(values, dist):
        perm = [
            (a * fb + (b + dist) % fb, a * fb + b) for a in range(fa) for b in range(fb)
        ]
        return lax.ppermute(values, "fs", perm)

    def from_a(values, dist):
        perm = [
            (((a + dist) % fa) * fb + b, a * fb + b) for a in range(fa) for b in range(fb)
        ]
        return lax.ppermute(values, "fs", perm)

    def from_chip(values, dist):
        perm = [
            (((z + dist) % chips) * cores + c, z * cores + c)
            for z in range(chips)
            for c in range(cores)
        ]
        return lax.ppermute(values, "tp", perm)

    def from_core(values):
        perm = [(i ^ 1, i) for i in range(tp_size)]
        return lax.ppermute(values, "tp", perm)

    def sum_fs(values):
        total = values
        for dist in range(1, fb):
            total = total + from_b(values, dist)
        whole = total
        for dist in range(1, fa):
            whole = whole + from_a(total, dist)
        return whole

    def sum_tp(values):
        total = values + from_core(values) if cores == 2 else values
        whole = total
        for dist in range(1, chips):
            whole = whole + from_chip(total, dist)
        return whole

    def local(tokens, up_gate, up_val, gate_weight, val_weight, gate_taps, val_taps, hidden_grad):
        fs_at = lax.axis_index("fs")
        tp_at = lax.axis_index("tp")
        a_at, b_at = fs_at // fb, fs_at % fb
        z_at, c_at = tp_at // cores, tp_at % cores
        rows, hidden = up_gate.shape
        shard, width = tokens.shape
        block = width // fs_size
        wide = fa * block
        taps = gate_taps.shape[0]
        step = hidden // CHUNKS

        def columns(dist):
            parts = []
            for d in range(fa):
                start = (((a_at + d) % fa) * fb + (b_at + dist) % fb) * block
                parts.append(lax.dynamic_slice(tokens, (0, start), (shard, block)))
            return jnp.concatenate(parts, axis=1)

        mine = [columns(0)]
        for dist in range(1, fb):
            mine.append(from_b(columns(fb - dist), dist))
        token_shard = jnp.stack(mine)

        def chunked(gate, val):
            parts = []
            for k in range(CHUNKS):
                cut = slice(k * step, (k + 1) * step)
                parts += [gate[cut], val[cut]]
            return jnp.concatenate(parts, axis=0)

        weights = [chunked(gate_weight.T, val_weight.T)]
        for d in range(1, fa):
            weights.append(from_a(weights[0], d))

        fields = (up_gate.T, up_val.T, hidden_grad.T)
        tap_fields = (gate_taps.T.astype(jnp.float32), val_taps.T.astype(jnp.float32))
        backs = [[] for _ in range(fb)]
        tap_parts = []
        for k in range(CHUNKS):
            back, tap = chunk_backs(k, step, *fields, *tap_fields)
            backs[0].append(back)
            tap_parts.append(tap)
            for d in range(1, fb):
                backs[d].append(from_b(back, d))

        pieces = [token_shard]
        for dist in range(1, chips):
            pieces.append(from_chip(token_shard, dist))
        pieces = jnp.stack(pieces)
        sides = [pieces] + ([from_core(pieces)] if cores == 2 else [])
        token_rows = []
        for d in range(fb):
            whole = jnp.zeros((tp_size, shard, wide), tokens.dtype)
            for side, held in enumerate(sides):
                core = (c_at + side) % cores
                for dist in range(chips):
                    place = ((z_at + dist) % chips) * cores + core
                    whole = lax.dynamic_update_slice(whole, held[dist, d][None], (place, 0, 0))
            token_rows.append(whole.reshape(rows, wide))

        tap_sums = sum_fs(jnp.concatenate(tap_parts, axis=0).T)
        taps_grad = tap_sums.reshape(2, taps, hidden)
        tap_norms = sum_tp(jnp.sum(taps_grad * taps_grad, axis=2))

        def dot(left, right, dims):
            return lax.dot_general(left, right, dims, preferred_element_type=jnp.float32)

        inner = (((1,), (0,)), ((), ()))
        over_hidden = (((0,), (0,)), ((), ()))

        def reduced(d):
            back = jnp.concatenate(backs[d], axis=0)
            part = jnp.concatenate(
                [dot(back, weight, over_hidden).astype(jnp.bfloat16) for weight in weights], axis=1
            ).reshape(chips, cores, shard, wide)

            def side(core):
                return lax.dynamic_slice_in_dim(part, core, 1, axis=1)[:, 0]

            if cores == 2:
                other = from_core(side(1 - c_at))
                total = side(c_at).astype(jnp.float32) + other.astype(jnp.float32)
                summed = total.astype(jnp.bfloat16)
            else:
                summed = part[:, 0]

            def chip(dist):
                return lax.dynamic_slice_in_dim(summed, (z_at + dist) % chips, 1, axis=0)[0]

            total = chip(0).astype(jnp.float32)
            for dist in range(1, chips):
                total = total + from_chip(chip(chips - dist), dist).astype(jnp.float32)
            return total.astype(jnp.bfloat16)

        own_rows = reduced(0)

        grads = []
        for k in range(CHUNKS):
            def partial(d_a):
                at = slice(d_a * block, (d_a + 1) * block)
                total = dot(backs[0][k], token_rows[0][:, at], inner)
                for d in range(1, fb):
                    total = total + dot(backs[d][k], token_rows[d][:, at], inner)
                return total

            sent = [partial(fa - d).astype(jnp.bfloat16) for d in range(1, fa)]
            total = partial(0)
            for d in range(1, fa):
                total = total + from_a(sent[d - 1], d).astype(jnp.float32)
            grads.append(total)
        gate_grad = jnp.concatenate([g[:step] for g in grads], axis=0)
        val_grad = jnp.concatenate([g[step:] for g in grads], axis=0)
        norms = sum_tp(
            jnp.stack(
                (jnp.sum(gate_grad * gate_grad, axis=0), jnp.sum(val_grad * val_grad, axis=0))
            )
        )

        placed = [own_rows]
        for d in range(1, fb):
            placed.append(from_b(reduced(fb - d), d))
        input_grad = jnp.zeros((shard, width), tokens.dtype)
        for d in range(fb):
            for d_a in range(fa):
                start = (((a_at + d_a) % fa) * fb + (b_at + d) % fb) * block
                input_grad = lax.dynamic_update_slice(
                    input_grad, placed[d][:, d_a * block : (d_a + 1) * block], (0, start)
                )
        return (
            input_grad,
            gate_grad.T,
            val_grad.T,
            taps_grad[0],
            taps_grad[1],
            norms[0],
            norms[1],
            tap_norms,
        )

    return local


def solution(mesh):
    in_specs = (
        P(("fs", "tp"), None),
        P("fs", "tp"),
        P("fs", "tp"),
        P("fs", "tp"),
        P("fs", "tp"),
        P(None, "tp"),
        P(None, "tp"),
        P("fs", "tp"),
    )
    out_specs = (
        P(("fs", "tp"), None),
        P("fs", "tp"),
        P("fs", "tp"),
        P(None, "tp"),
        P(None, "tp"),
        P("fs"),
        P("fs"),
        P(),
    )
    local = make_local(mesh.shape["fs"], mesh.shape["tp"])
    return jax.shard_map(local, mesh=mesh, in_specs=in_specs, out_specs=out_specs, check_vma=False)
```

profile of v0, /device:TPU:0, one launch (start us, length us, event | category | flops | bytes accessed | tf_op | source)
XLA Modules:
  0.0 277.0 jit_solution(9613992983966102492)
XLA Ops:
  3.8 6.0 %shard_map.143 = (bf16[352,1024]{1,0:T(8,128)(2,1)}, f32[176,6]{1,0:T(8,128)}) custom-call(bf16[704,1024]{1,0:T(8,128)(2,1)} %bitcast.145, bf16[704,1024]{1,0:T(8,128)(2,1)} %bitcast.149, bf16[704,1024]{1,0:T(8,128)(2,1)} %bitcast.153, f32[704,3]{1,0:T(8,128)} %bitcast.165, f32[704,3]{1,0:T(8,128)} %bitcast.169), custom_call_target="tpu_custom_call" | custom-call | flops 10813440 | bytes 1802240 | tf_op jit(solution)/shard_map/pallas_call | solution.py:72
  9.8 6.0 %shard_map.144 = (bf16[352,1024]{1,0:T(8,128)(2,1)}, f32[176,6]{1,0:T(8,128)}) custom-call(bf16[704,1024]{1,0:T(8,128)(2,1)} %bitcast.146, bf16[704,1024]{1,0:T(8,128)(2,1)} %bitcast.150, bf16[704,1024]{1,0:T(8,128)(2,1)} %bitcast.154, f32[704,3]{1,0:T(8,128)} %bitcast.166, f32[704,3]{1,0:T(8,128)} %bitcast.170), custom_call_target="tpu_custom_call" | custom-call | flops 10813440 | bytes 1802240 | tf_op jit(solution)/shard_map/pallas_call | solution.py:72
  15.8 6.0 %shard_map.145 = (bf16[352,1024]{1,0:T(8,128)(2,1)}, f32[176,6]{1,0:T(8,128)}) custom-call(bf16[704,1024]{1,0:T(8,128)(2,1)} %bitcast.147, bf16[704,1024]{1,0:T(8,128)(2,1)} %bitcast.151, bf16[704,1024]{1,0:T(8,128)(2,1)} %bitcast.155, f32[704,3]{1,0:T(8,128)} %bitcast.167, f32[704,3]{1,0:T(8,128)} %bitcast.171), custom_call_target="tpu_custom_call" | custom-call | flops 10813440 | bytes 1802240 | tf_op jit(solution)/shard_map/pallas_call | solution.py:72
  21.8 6.1 %shard_map.146 = (bf16[352,1024]{1,0:T(8,128)(2,1)}, f32[176,6]{1,0:T(8,128)}) custom-call(bf16[704,1024]{1,0:T(8,128)(2,1)} %bitcast.148, bf16[704,1024]{1,0:T(8,128)(2,1)} %bitcast.152, bf16[704,1024]{1,0:T(8,128)(2,1)} %bitcast.156, f32[704,3]{1,0:T(8,128)} %bitcast.168, f32[704,3]{1,0:T(8,128)} %bitcast.172), custom_call_target="tpu_custom_call" | custom-call | flops 10813440 | bytes 1802240 | tf_op jit(solution)/shard_map/pallas_call | solution.py:72
  51.4 3.6 %collective-permute-start.30 = (f32[2,3]{1,0:T(2,128)S(1)}, f32[2,3]{1,0:T(2,128)S(1)}, u32[]{:S(2)}, u32[]{:S(2)}) collective-permute-start(f32[2,3]{1,0:T(2,128)S(1)} %add.398), channel_id=1, source_target_pairs={{2,0},{3,1},{4,2},{5,3},{6,4},{7,5},{0,6},{1,7},{10,8},{11,9},{12,... | collective-permute-start | bytes 80 | tf_op jit(solution)/shard_map/ppermute | solution.py:115
  62.5 3.9 %collective-permute-done.32 = f32[2,3]{1,0:T(2,128)S(1)} collective-permute-done((f32[2,3]{1,0:T(2,128)S(1)}, f32[2,3]{1,0:T(2,128)S(1)}, u32[]{:S(2)}, u32[]{:S(2)}) %collective-permute-start.32) | collective-permute-done | bytes 56 | tf_op jit(solution)/shard_map/ppermute | solution.py:115
  76.0 12.8 %collective-permute-done.7 = bf16[352,1024]{1,0:T(8,128)(2,1)S(1)} collective-permute-done((bf16[352,1024]{1,0:T(8,128)(2,1)}, bf16[352,1024]{1,0:T(8,128)(2,1)S(1)}, u32[]{:S(2)}, u32[]{:S(2)}) %collective-permute-start.7) | collective-permute-done | bytes 720928 | tf_op jit(solution)/shard_map/ppermute | solution.py:101
  90.4 12.4 %collective-permute-done.8 = bf16[352,1024]{1,0:T(8,128)(2,1)S(1)} collective-permute-done((bf16[352,1024]{1,0:T(8,128)(2,1)}, bf16[352,1024]{1,0:T(8,128)(2,1)S(1)}, u32[]{:S(2)}, u32[]{:S(2)}) %collective-permute-start.8) | collective-permute-done | bytes 720928 | tf_op jit(solution)/shard_map/ppermute | solution.py:101
  109.0 3.2 %reshape.43 = bf16[4,2,128,1024]{2,1,0,3:T(2,128)(2,1)S(1)} reshape(bf16[1024,1024]{0,1:T(8,128)(2,1)} %pad_maximum_fusion.1) | data formatting | bytes 4194304 | tf_op jit(solution)/shard_map/reshape | solution.py:212
  112.3 4.1 %convolution_convert_fusion.2 = bf16[1024,512]{0,1:T(8,128)(2,1)S(1)} fusion(bf16[1408,1024]{1,0:T(8,128)(2,1)} %copy-done.17, bf16[1408,512]{1,0:T(8,128)(2,1)} %copy-done.23), kind=kOutput, calls=%fused_computation.9 | convolution fusion | flops 1476919296 | bytes 5373952 | tf_op jit(solution)/shard_map/dot_general | solution.py:203
  117.9 4.5 %reshape.42 = bf16[4,2,128,1024]{2,1,0,3:T(2,128)(2,1)} reshape(bf16[1024,1024]{0,1:T(8,128)(2,1)} %pad_maximum_fusion) | data formatting | bytes 4194304 | tf_op jit(solution)/shard_map/reshape | solution.py:212
  122.4 11.4 %constant_dynamic-slice_fusion.5 = (bf16[4,1,128,1024]{2,1,0,3:T(2,128)(2,1)}, bf16[4,1,128,1024]{2,1,0,3:T(2,128)(2,1)}, bf16[4,1,128,1024]{2,1,0,3:T(2,128)(2,1)}, bf16[4,1,128,1024]{2,1,0,3:T(2,128)(2,1)}) fusion(bf16[4,2,128,1024]{2,1,0,3:T(2,128)(2,1)S(1)} %reshape.43, s32[]{:T(128)S(6)} %select_n.199, s32[]{:T(128)S(6)} %select_n.200, ...), kind=kLoop, calls=%fused_computation.133 | loop fusion | bytes 8388616 | tf_op jit(solution)/shard_map/dynamic_slice | solution.py:215
  133.8 5.8 %copy.29 = bf16[4,1,128,1024]{3,2,0,1:T(8,128)(2,1)} copy(bf16[4,1,128,1024]{2,1,0,3:T(2,128)(2,1)} %get-tuple-element.41) | data formatting | bytes 2097152 | tf_op jit(solution)/shard_map/dynamic_slice | solution.py:215
  141.2 5.8 %copy.27 = bf16[4,1,128,1024]{3,2,0,1:T(8,128)(2,1)} copy(bf16[4,1,128,1024]{2,1,0,3:T(2,128)(2,1)} %get-tuple-element.78) | data formatting | bytes 2097152 | tf_op jit(solution)/shard_map/dynamic_slice | solution.py:215
  154.1 5.8 %copy.35 = bf16[4,1,128,1024]{3,2,0,1:T(8,128)(2,1)} copy(bf16[4,1,128,1024]{2,1,0,3:T(2,128)(2,1)} %get-tuple-element.40) | data formatting | bytes 2097152
  159.9 4.6 %copy.34 = bf16[4,1,128,1024]{3,2,0,1:T(8,128)(2,1)S(1)} copy(bf16[4,1,128,1024]{2,1,0,3:T(2,128)(2,1)} %get-tuple-element.79) | data formatting | bytes 2097152
  166.5 3.6 %collective-permute-start.10 = (bf16[128,1024]{1,0:T(8,128)(2,1)S(1)}, bf16[128,1024]{1,0:T(8,128)(2,1)S(1)}, u32[]{:S(2)}, u32[]{:S(2)}) collective-permute-start(bf16[128,1024]{1,0:T(8,128)(2,1)S(1)} %get-tuple-element.48), channel_id=1, source_target_pairs={{2,0},{3,1},{4,2},{5,3},{6,4},{7,5},{0,6},{1,7},{10,8},{11,9},{12,... | collective-permute-start | bytes 786440 | tf_op jit(solution)/shard_map/ppermute | solution.py:115
  178.3 15.3 %collective-permute-done.11 = bf16[128,1024]{1,0:T(8,128)(2,1)S(1)} collective-permute-done((bf16[128,1024]{1,0:T(8,128)(2,1)S(1)}, bf16[128,1024]{1,0:T(8,128)(2,1)S(1)}, u32[]{:S(2)}, u32[]{:S(2)}) %collective-permute-start.11) | collective-permute-done | bytes 262176 | tf_op jit(solution)/shard_map/ppermute | solution.py:115
  195.6 20.0 %collective-permute-done.3 = bf16[128,1024]{1,0:T(8,128)(2,1)S(1)} collective-permute-done((bf16[128,1024]{1,0:T(8,128)(2,1)S(1)}, bf16[128,1024]{1,0:T(8,128)(2,1)S(1)}, u32[]{:S(2)}, u32[]{:S(2)}) %collective-permute-start.3) | collective-permute-done | bytes 262176 | tf_op jit(solution)/shard_map/ppermute | solution.py:115
  238.8 3.7 %collective-permute-done.19 = bf16[352,512]{1,0:T(8,128)(2,1)S(1)} collective-permute-done((bf16[352,512]{1,0:T(8,128)(2,1)S(1)}, bf16[352,512]{1,0:T(8,128)(2,1)S(1)}, u32[]{:S(2)}, u32[]{:S(2)}) %collective-permute-start.19) | collective-permute-done | bytes 360480 | tf_op jit(solution)/shard_map/ppermute | solution.py:107
  243.1 7.1 %collective-permute-done.20 = bf16[352,512]{1,0:T(8,128)(2,1)S(1)} collective-permute-done((bf16[352,512]{1,0:T(8,128)(2,1)S(1)}, bf16[352,512]{1,0:T(8,128)(2,1)S(1)}, u32[]{:S(2)}, u32[]{:S(2)}) %collective-permute-start.20) | collective-permute-done | bytes 360480 | tf_op jit(solution)/shard_map/ppermute | solution.py:107
  250.8 7.2 %collective-permute-done.21 = bf16[352,512]{1,0:T(8,128)(2,1)S(1)} collective-permute-done((bf16[352,512]{1,0:T(8,128)(2,1)S(1)}, bf16[352,512]{1,0:T(8,128)(2,1)S(1)}, u32[]{:S(2)}, u32[]{:S(2)}) %collective-permute-start.21) | collective-permute-done | bytes 360480 | tf_op jit(solution)/shard_map/ppermute | solution.py:107
  258.6 5.7 %collective-permute-done.22 = bf16[352,512]{1,0:T(8,128)(2,1)S(1)} collective-permute-done((bf16[352,512]{1,0:T(8,128)(2,1)S(1)}, bf16[352,512]{1,0:T(8,128)(2,1)S(1)}, u32[]{:S(2)}, u32[]{:S(2)}) %collective-permute-start.22) | collective-permute-done | bytes 360480 | tf_op jit(solution)/shard_map/ppermute | solution.py:107
  272.9 3.4 %collective-permute-done.28 = f32[2,512]{1,0:T(2,128)S(1)} collective-permute-done((f32[2,512]{1,0:T(2,128)S(1)}, f32[2,512]{1,0:T(2,128)S(1)}, u32[]{:S(2)}, u32[]{:S(2)}) %collective-permute-start.28) | collective-permute-done | bytes 4128 | tf_op jit(solution)/shard_map/ppermute | solution.py:115
  (189 shorter events, 107.3 us)
Async XLA Ops:
  29.3 16.9 %collective-permute-start.23 = (f32[6,704]{1,0:T(8,128)S(1)}, f32[6,704]{1,0:T(8,128)S(1)}, u32[]{:S(2)}, u32[]{:S(2)}) collective-permute-start(f32[6,704]{1,0:T(8,128)S(1)} %maximum_bitcast_fusion.1), channel_id=1, source_target_pairs={{8,0},{0,8},{24,16},{16,24},{9,1},{1,9},{25,17},{17,25},{10,2},{2,... | collective-permute-start | bytes 50696 | tf_op jit(solution)/shard_map/ppermute | solution.py:101
  33.0 35.5 %collective-permute-start.14 = (bf16[128,1024]{1,0:T(8,128)(2,1)}, bf16[128,1024]{1,0:T(8,128)(2,1)}, u32[]{:S(2)}, u32[]{:S(2)}) collective-permute-start(bf16[128,1024]{1,0:T(8,128)(2,1)} %pad_maximum_fusion.6), channel_id=1, source_target_pairs={{8,0},{0,8},{24,16},{16,24},{9,1},{1,9},{25,17},{17,25},{10,2},{2,... | collective-permute-start | bytes 786440 | tf_op jit(solution)/shard_map/ppermute | solution.py:101
  33.2 38.3 %collective-permute-start.5 = (bf16[352,1024]{1,0:T(8,128)(2,1)}, bf16[352,1024]{1,0:T(8,128)(2,1)S(1)}, u32[]{:S(2)}, u32[]{:S(2)}) collective-permute-start(bf16[352,1024]{1,0:T(8,128)(2,1)} %get-tuple-element.16), channel_id=1, source_target_pairs={{8,0},{0,8},{24,16},{16,24},{9,1},{1,9},{25,17},{17,25},{10,2},{2,... | collective-permute-start | bytes 2162696 | tf_op jit(solution)/shard_map/ppermute | solution.py:101
  35.1 38.5 %collective-permute-start.6 = (bf16[352,1024]{1,0:T(8,128)(2,1)}, bf16[352,1024]{1,0:T(8,128)(2,1)S(1)}, u32[]{:S(2)}, u32[]{:S(2)}) collective-permute-start(bf16[352,1024]{1,0:T(8,128)(2,1)} %get-tuple-element.17), channel_id=1, source_target_pairs={{8,0},{0,8},{24,16},{16,24},{9,1},{1,9},{25,17},{17,25},{10,2},{2,... | collective-permute-start | bytes 2162696 | tf_op jit(solution)/shard_map/ppermute | solution.py:101
  35.2 53.6 %collective-permute-start.7 = (bf16[352,1024]{1,0:T(8,128)(2,1)}, bf16[352,1024]{1,0:T(8,128)(2,1)S(1)}, u32[]{:S(2)}, u32[]{:S(2)}) collective-permute-start(bf16[352,1024]{1,0:T(8,128)(2,1)} %get-tuple-element.18), channel_id=1, source_target_pairs={{8,0},{0,8},{24,16},{16,24},{9,1},{1,9},{25,17},{17,25},{10,2},{2,... | collective-permute-start | bytes 2162696 | tf_op jit(solution)/shard_map/ppermute | solution.py:101
  66.4 39.2 %collective-permute-start = (bf16[1408,512]{1,0:T(8,128)(2,1)}, bf16[1408,512]{1,0:T(8,128)(2,1)S(1)}, u32[]{:S(2)}, u32[]{:S(2)}) collective-permute-start(bf16[1408,512]{1,0:T(8,128)(2,1)} %copy-done.21), channel_id=1, source_target_pairs={{16,0},{24,8},{0,16},{8,24},{17,1},{25,9},{1,17},{9,25},{18,2},{26... | collective-permute-start | bytes 4325384 | tf_op jit(solution)/shard_map/ppermute | solution.py:107
  68.5 34.3 %collective-permute-start.8 = (bf16[352,1024]{1,0:T(8,128)(2,1)}, bf16[352,1024]{1,0:T(8,128)(2,1)S(1)}, u32[]{:S(2)}, u32[]{:S(2)}) collective-permute-start(bf16[352,1024]{1,0:T(8,128)(2,1)} %get-tuple-element.19), channel_id=1, source_target_pairs={{8,0},{0,8},{24,16},{16,24},{9,1},{1,9},{25,17},{17,25},{10,2},{2,... | collective-permute-start | bytes 2162696 | tf_op jit(solution)/shard_map/ppermute | solution.py:101
  71.5 76.1 %collective-permute-start.15 = (bf16[2,128,1024]{2,1,0:T(8,128)(2,1)}, bf16[2,128,1024]{2,1,0:T(8,128)(2,1)}, u32[]{:S(2)}, u32[]{:S(2)}) collective-permute-start(bf16[2,128,1024]{2,1,0:T(8,128)(2,1)} %get-tuple-element.68), channel_id=1, source_target_pairs={{2,0},{3,1},{4,2},{5,3},{6,4},{7,5},{0,6},{1,7},{10,8},{11,9},{12,... | collective-permute-start | bytes 1572872 | tf_op jit(solution)/shard_map/ppermute | solution.py:115
  73.6 74.0 %collective-permute-start.16 = (bf16[2,128,1024]{2,1,0:T(8,128)(2,1)}, bf16[2,128,1024]{2,1,0:T(8,128)(2,1)}, u32[]{:S(2)}, u32[]{:S(2)}) collective-permute-start(bf16[2,128,1024]{2,1,0:T(8,128)(2,1)} %get-tuple-element.68), channel_id=1, source_target_pairs={{4,0},{5,1},{6,2},{7,3},{0,4},{1,5},{2,6},{3,7},{12,8},{13,9},{14,... | collective-permute-start | bytes 1572872 | tf_op jit(solution)/shard_map/ppermute | solution.py:115
  88.8 58.8 %collective-permute-start.17 = (bf16[2,128,1024]{2,1,0:T(8,128)(2,1)}, bf16[2,128,1024]{2,1,0:T(8,128)(2,1)}, u32[]{:S(2)}, u32[]{:S(2)}) collective-permute-start(bf16[2,128,1024]{2,1,0:T(8,128)(2,1)} %get-tuple-element.68), channel_id=1, source_target_pairs={{6,0},{7,1},{0,2},{1,3},{2,4},{3,5},{4,6},{5,7},{14,8},{15,9},{8,1... | collective-permute-start | bytes 1572872 | tf_op jit(solution)/shard_map/ppermute | solution.py:115
  139.6 24.9 %collective-permute-start.9 = (bf16[4,128,1024]{2,1,0:T(8,128)(2,1)}, bf16[4,128,1024]{2,1,0:T(8,128)(2,1)}, u32[]{:S(2)}, u32[]{:S(2)}) collective-permute-start(bf16[4,128,1024]{2,1,0:T(8,128)(2,1)} %bitcast.14), channel_id=1, source_target_pairs={{1,0},{0,1},{3,2},{2,3},{5,4},{4,5},{7,6},{6,7},{9,8},{8,9},{11,10... | collective-permute-start | bytes 3145736 | tf_op jit(solution)/shard_map/ppermute | solution.py:119
  147.0 24.1 %collective-permute-start.1 = (bf16[4,128,1024]{2,1,0:T(8,128)(2,1)}, bf16[4,128,1024]{2,1,0:T(8,128)(2,1)}, u32[]{:S(2)}, u32[]{:S(2)}) collective-permute-start(bf16[4,128,1024]{2,1,0:T(8,128)(2,1)} %bitcast.181), channel_id=1, source_target_pairs={{1,0},{0,1},{3,2},{2,3},{5,4},{4,5},{7,6},{6,7},{9,8},{8,9},{11,10... | collective-permute-start | bytes 3145736 | tf_op jit(solution)/shard_map/ppermute | solution.py:119
  150.5 65.4 %collective-permute-start.18 = (bf16[4,2,128,1024]{3,2,1,0:T(8,128)(2,1)}, bf16[4,2,128,1024]{3,2,1,0:T(8,128)(2,1)}, u32[]{:S(2)}, u32[]{:S(2)}) collective-permute-start(bf16[4,2,128,1024]{3,2,1,0:T(8,128)(2,1)} %pad_maximum_fusion.2), channel_id=1, source_target_pairs={{1,0},{0,1},{3,2},{2,3},{5,4},{4,5},{7,6},{6,7},{9,8},{8,9},{11,10... | collective-permute-start | bytes 6291464 | tf_op jit(solution)/shard_map/ppermute | solution.py:119
  166.5 10.4 %collective-permute-start.10 = (bf16[128,1024]{1,0:T(8,128)(2,1)S(1)}, bf16[128,1024]{1,0:T(8,128)(2,1)S(1)}, u32[]{:S(2)}, u32[]{:S(2)}) collective-permute-start(bf16[128,1024]{1,0:T(8,128)(2,1)S(1)} %get-tuple-element.48), channel_id=1, source_target_pairs={{2,0},{3,1},{4,2},{5,3},{6,4},{7,5},{0,6},{1,7},{10,8},{11,9},{12,... | collective-permute-start | bytes 786440 | tf_op jit(solution)/shard_map/ppermute | solution.py:115
  170.1 23.5 %collective-permute-start.11 = (bf16[128,1024]{1,0:T(8,128)(2,1)S(1)}, bf16[128,1024]{1,0:T(8,128)(2,1)S(1)}, u32[]{:S(2)}, u32[]{:S(2)}) collective-permute-start(bf16[128,1024]{1,0:T(8,128)(2,1)S(1)} %get-tuple-element.50), channel_id=1, source_target_pairs={{4,0},{5,1},{6,2},{7,3},{0,4},{1,5},{2,6},{3,7},{12,8},{13,9},{14,... | collective-permute-start | bytes 786440 | tf_op jit(solution)/shard_map/ppermute | solution.py:115
  170.1 24.6 %collective-permute-start.12 = (bf16[128,1024]{1,0:T(8,128)(2,1)S(1)}, bf16[128,1024]{1,0:T(8,128)(2,1)S(1)}, u32[]{:S(2)}, u32[]{:S(2)}) collective-permute-start(bf16[128,1024]{1,0:T(8,128)(2,1)S(1)} %get-tuple-element.49), channel_id=1, source_target_pairs={{6,0},{7,1},{0,2},{1,3},{2,4},{3,5},{4,6},{5,7},{14,8},{15,9},{8,1... | collective-permute-start | bytes 786440 | tf_op jit(solution)/shard_map/ppermute | solution.py:115
  172.9 22.8 %collective-permute-start.2 = (bf16[128,1024]{1,0:T(8,128)(2,1)S(1)}, bf16[128,1024]{1,0:T(8,128)(2,1)S(1)}, u32[]{:S(2)}, u32[]{:S(2)}) collective-permute-start(bf16[128,1024]{1,0:T(8,128)(2,1)S(1)} %get-tuple-element.51), channel_id=1, source_target_pairs={{2,0},{3,1},{4,2},{5,3},{6,4},{7,5},{0,6},{1,7},{10,8},{11,9},{12,... | collective-permute-start | bytes 786440 | tf_op jit(solution)/shard_map/ppermute | solution.py:115
  176.9 38.7 %collective-permute-start.3 = (bf16[128,1024]{1,0:T(8,128)(2,1)S(1)}, bf16[128,1024]{1,0:T(8,128)(2,1)S(1)}, u32[]{:S(2)}, u32[]{:S(2)}) collective-permute-start(bf16[128,1024]{1,0:T(8,128)(2,1)S(1)} %get-tuple-element.53), channel_id=1, source_target_pairs={{4,0},{5,1},{6,2},{7,3},{0,4},{1,5},{2,6},{3,7},{12,8},{13,9},{14,... | collective-permute-start | bytes 786440 | tf_op jit(solution)/shard_map/ppermute | solution.py:115
  193.6 22.0 %collective-permute-start.4 = (bf16[128,1024]{1,0:T(8,128)(2,1)S(1)}, bf16[128,1024]{1,0:T(8,128)(2,1)S(1)}, u32[]{:S(2)}, u32[]{:S(2)}) collective-permute-start(bf16[128,1024]{1,0:T(8,128)(2,1)S(1)} %get-tuple-element.52), channel_id=1, source_target_pairs={{6,0},{7,1},{0,2},{1,3},{2,4},{3,5},{4,6},{5,7},{14,8},{15,9},{8,1... | collective-permute-start | bytes 786440 | tf_op jit(solution)/shard_map/ppermute | solution.py:115
  194.9 72.2 %collective-permute-start.13 = (bf16[128,1024]{1,0:T(8,128)(2,1)S(1)}, bf16[128,1024]{1,0:T(8,128)(2,1)S(1)}, u32[]{:S(2)}, u32[]{:S(2)}) collective-permute-start(bf16[128,1024]{1,0:T(8,128)(2,1)S(1)} %fusion.38), channel_id=1, source_target_pairs={{8,0},{0,8},{24,16},{16,24},{9,1},{1,9},{25,17},{17,25},{10,2},{2,... | collective-permute-start | bytes 786440 | tf_op jit(solution)/shard_map/ppermute | solution.py:101
  231.2 11.4 %collective-permute-start.19 = (bf16[352,512]{1,0:T(8,128)(2,1)S(1)}, bf16[352,512]{1,0:T(8,128)(2,1)S(1)}, u32[]{:S(2)}, u32[]{:S(2)}) collective-permute-start(bf16[352,512]{1,0:T(8,128)(2,1)S(1)} %fusion.6), channel_id=1, source_target_pairs={{16,0},{24,8},{0,16},{8,24},{17,1},{25,9},{1,17},{9,25},{18,2},{26... | collective-permute-start | bytes 1081352 | tf_op jit(solution)/shard_map/ppermute | solution.py:107
  233.3 16.9 %collective-permute-start.20 = (bf16[352,512]{1,0:T(8,128)(2,1)S(1)}, bf16[352,512]{1,0:T(8,128)(2,1)S(1)}, u32[]{:S(2)}, u32[]{:S(2)}) collective-permute-start(bf16[352,512]{1,0:T(8,128)(2,1)S(1)} %fusion.7), channel_id=1, source_target_pairs={{16,0},{24,8},{0,16},{8,24},{17,1},{25,9},{1,17},{9,25},{18,2},{26... | collective-permute-start | bytes 1081352 | tf_op jit(solution)/shard_map/ppermute | solution.py:107
  234.4 23.5 %collective-permute-start.21 = (bf16[352,512]{1,0:T(8,128)(2,1)S(1)}, bf16[352,512]{1,0:T(8,128)(2,1)S(1)}, u32[]{:S(2)}, u32[]{:S(2)}) collective-permute-start(bf16[352,512]{1,0:T(8,128)(2,1)S(1)} %fusion.8), channel_id=1, source_target_pairs={{16,0},{24,8},{0,16},{8,24},{17,1},{25,9},{1,17},{9,25},{18,2},{26... | collective-permute-start | bytes 1081352 | tf_op jit(solution)/shard_map/ppermute | solution.py:107
  236.6 27.8 %collective-permute-start.22 = (bf16[352,512]{1,0:T(8,128)(2,1)S(1)}, bf16[352,512]{1,0:T(8,128)(2,1)S(1)}, u32[]{:S(2)}, u32[]{:S(2)}) collective-permute-start(bf16[352,512]{1,0:T(8,128)(2,1)S(1)} %fusion.9), channel_id=1, source_target_pairs={{16,0},{24,8},{0,16},{8,24},{17,1},{25,9},{1,17},{9,25},{18,2},{26... | collective-permute-start | bytes 1081352 | tf_op jit(solution)/shard_map/ppermute | solution.py:107
  (33 other events, 238.0 us)
where the time goes:
time: 279 us; the launch traced here: 277 us
  waiting for transfers between devices  102 us (37%)
  local copies, waits for them, and re-layouts  65.8 us (24%)
  starting transfers between devices  42.4 us (15%)
  matrix products  26.1 us (9%)
  Pallas kernels  24.1 us (9%)
  other arithmetic  15.3 us (5%)
    ppermute x15, waiting for transfers between devices, from_chip(): return lax.ppermute(values, 'tp', perm)  48.3 us
    dot_general x20, matrix products, dot(): lax.dot_general(left, right, dims, preferred_element_type=jnp.float32)  26.1 us
    ppermute x15, starting transfers between devices, from_chip(): return lax.ppermute(values, 'tp', perm)  26.1 us
    ppermute x6, waiting for transfers between devices, from_a(): return lax.ppermute(values, 'fs', perm)  25.9 us
    ppermute x7, waiting for transfers between devices, from_b(): return lax.ppermute(values, 'fs', perm)  25.2 us
    pallas_call x4, Pallas kernels, chunk_backs(): pl.pallas_call(functools.partial(backs_kernel, group), grid=(1,), in_spec...  24.1 us
    dynamic_slice x3, local copies, waits for them, and re-layouts, side(): return lax.dynamic_slice_in_dim(part, core, 1, axis=1)[:, 0]  23 us
    unnamed x63, local copies, waits for them, and re-layouts  17.4 us
  transfers between devices with their start and end apart: 33, of which 16 were waited for; matrix products, arithmetic and copies ran while one was open for 36% of the time, Pallas kernels for 0%

commit v1 on v0

--- a/solution.py
+++ b/solution.py
@@ -11,15 +11,15 @@
 CHUNKS = 4
 
 
-def backs_kernel(group, gate_ref, val_ref, grad_ref, gate_tap_ref, val_tap_ref, back_ref, tap_ref):
+def backs_kernel(group, gate_ref, val_ref, grad_ref, kernel_ref, back_ref, tap_ref):
     step, rows = gate_ref.shape
-    taps = gate_tap_ref.shape[1]
+    taps = kernel_ref.shape[1] // 2
     place = lax.broadcasted_iota(jnp.int32, (group, rows), 1) % SEQ
 
     def one(index, carry):
         at = pl.ds(pl.multiple_of(index * group, group), group)
-        gate_kernel = gate_tap_ref[at, :]
-        val_kernel = val_tap_ref[at, :]
+        gate_kernel = kernel_ref[at, 0:taps]
+        val_kernel = kernel_ref[at, taps : 2 * taps]
 
         def delayed(field, shift):
             if shift == 0:
@@ -63,16 +63,16 @@
     lax.fori_loop(0, step // group, one, 0)
 
 
-def chunk_backs(k, step, up_gate, up_val, hidden_grad, gate_taps, val_taps):
+def chunk_backs(k, step, up_gate, up_val, hidden_grad, kernels):
     rows = up_gate.shape[1]
-    taps = gate_taps.shape[1]
+    taps = kernels.shape[1] // 2
     group = 16 if step % 16 == 0 else 8
     field = pl.BlockSpec((step, rows), lambda i: (k, 0))
-    tap = pl.BlockSpec((step, taps), lambda i: (k, 0))
+    tap = pl.BlockSpec((step, 2 * taps), lambda i: (k, 0))
     return pl.pallas_call(
         functools.partial(backs_kernel, group),
         grid=(1,),
-        in_specs=[field, field, field, tap, tap],
+        in_specs=[field, field, field, tap],
         out_specs=[
             pl.BlockSpec((2 * step, rows), lambda i: (0, 0)),
             pl.BlockSpec((step, 2 * taps), lambda i: (0, 0)),
@@ -84,7 +84,60 @@
         cost_estimate=pl.CostEstimate(
             flops=60 * step * rows, bytes_accessed=10 * step * rows, transcendentals=step * rows
         ),
-    )(up_gate, up_val, hidden_grad, gate_taps, val_taps)
+    )(up_gate, up_val, hidden_grad, kernels)
+
+
+def rows_kernel(chunks, fa, chips, cores, at_ref, *refs):
+    back_refs = refs[:chunks]
+    gate_refs = refs[chunks : chunks + fa]
+    val_refs = refs[chunks + fa : chunks + 2 * fa]
+    out_ref = refs[-1]
+    shard = out_ref.shape[2]
+    block = gate_refs[0].shape[1]
+    step = back_refs[0].shape[0] // 2
+    over_hidden = (((0,), (0,)), ((), ()))
+
+    def one(chip, carry):
+        span = cores * shard
+        at = pl.ds(pl.multiple_of(chip * span, span), span)
+        place = lax.rem(chip - at_ref[0] + chips, chips)
+        for d in range(fa):
+            total = jnp.zeros((span, block), jnp.float32)
+            for k in range(chunks):
+                back = back_refs[k][:, at]
+                cut = slice(k * step, (k + 1) * step)
+                weight = jnp.concatenate((gate_refs[d][cut, :], val_refs[d][cut, :]), axis=0)
+                total = total + lax.dot_general(
+                    back, weight, over_hidden, preferred_element_type=jnp.float32
+                )
+            total = total.astype(jnp.bfloat16)
+            for core in range(cores):
+                side = lax.rem(at_ref[1] + core, cores)
+                out_ref[side, place, :, d * block : (d + 1) * block] = total[
+                    core * shard : (core + 1) * shard
+                ]
+        return carry
+
+    lax.fori_loop(0, chips, one, 0)
+
+
+def partial_rows(place, backs, gate_parts, val_parts, chips, cores):
+    rows = backs[0].shape[1]
+    shard = rows // (chips * cores)
+    fa = len(gate_parts)
+    hidden, block = gate_parts[0].shape
+    vmem = pl.BlockSpec(memory_space=pltpu.VMEM)
+    return pl.pallas_call(
+        functools.partial(rows_kernel, len(backs), fa, chips, cores),
+        in_specs=[pl.BlockSpec(memory_space=pltpu.SMEM)] + [vmem] * (len(backs) + 2 * fa),
+        out_specs=vmem,
+        out_shape=jax.ShapeDtypeStruct((cores, chips, shard, fa * block), jnp.bfloat16),
+        cost_estimate=pl.CostEstimate(
+            flops=4 * rows * hidden * fa * block,
+            bytes_accessed=4 * hidden * (rows + fa * block) + 2 * rows * fa * block,
+            transcendentals=0,
+        ),
+    )(place, *backs, *gate_parts, *val_parts)
 
 
 def make_local(fs_size, tp_size):
@@ -144,7 +197,8 @@
         block = width // fs_size
         wide = fa * block
         taps = gate_taps.shape[0]
-        step = hidden // CHUNKS
+        chunks = max(c for c in range(1, CHUNKS + 1) if hidden % (16 * c) == 0)
+        step = hidden // chunks
 
         def columns(dist):
             parts = []
@@ -158,23 +212,17 @@
             mine.append(from_b(columns(fb - dist), dist))
         token_shard = jnp.stack(mine)
 
-        def chunked(gate, val):
-            parts = []
-            for k in range(CHUNKS):
-                cut = slice(k * step, (k + 1) * step)
-                parts += [gate[cut], val[cut]]
-            return jnp.concatenate(parts, axis=0)
-
-        weights = [chunked(gate_weight.T, val_weight.T)]
+        gate_parts, val_parts = [gate_weight.T], [val_weight.T]
         for d in range(1, fa):
-            weights.append(from_a(weights[0], d))
+            gate_parts.append(from_a(gate_parts[0], d))
+            val_parts.append(from_a(val_parts[0], d))
 
         fields = (up_gate.T, up_val.T, hidden_grad.T)
-        tap_fields = (gate_taps.T.astype(jnp.float32), val_taps.T.astype(jnp.float32))
+        kernels = jnp.concatenate((gate_taps, val_taps), axis=0).astype(jnp.float32).T
         backs = [[] for _ in range(fb)]
         tap_parts = []
-        for k in range(CHUNKS):
-            back, tap = chunk_backs(k, step, *fields, *tap_fields)
+        for k in range(chunks):
+            back, tap = chunk_backs(k, step, *fields, kernels)
             backs[0].append(back)
             tap_parts.append(tap)
             for d in range(1, fb):
@@ -203,26 +251,21 @@
             return lax.dot_general(left, right, dims, preferred_element_type=jnp.float32)
 
         inner = (((1,), (0,)), ((), ()))
-        over_hidden = (((0,), (0,)), ((), ()))
 
         def reduced(d):
-            back = jnp.concatenate(backs[d], axis=0)
-            part = jnp.concatenate(
-                [dot(back, weight, over_hidden).astype(jnp.bfloat16) for weight in weights], axis=1
-            ).reshape(chips, cores, shard, wide)
-
-            def side(core):
-                return lax.dynamic_slice_in_dim(part, core, 1, axis=1)[:, 0]
-
+            part = partial_rows(
+                jnp.stack((z_at, c_at)).astype(jnp.int32),
+                backs[d], gate_parts, val_parts, chips, cores,
+            )
             if cores == 2:
-                other = from_core(side(1 - c_at))
-                total = side(c_at).astype(jnp.float32) + other.astype(jnp.float32)
+                other = from_core(part[1])
+                total = part[0].astype(jnp.float32) + other.astype(jnp.float32)
                 summed = total.astype(jnp.bfloat16)
             else:
-                summed = part[:, 0]
+                summed = part[0]
 
             def chip(dist):
-                return lax.dynamic_slice_in_dim(summed, (z_at + dist) % chips, 1, axis=0)[0]
+                return summed[dist]
 
             total = chip(0).astype(jnp.float32)
             for dist in range(1, chips):
@@ -232,7 +275,7 @@
         own_rows = reduced(0)
 
         grads = []
-        for k in range(CHUNKS):
+        for k in range(chunks):
             def partial(d_a):
                 at = slice(d_a * block, (d_a + 1) * block)
                 total = dot(backs[0][k], token_rows[0][:, at], inner)
@@ -250,7 +293,7 @@
         norms = sum_tp(
             jnp.stack(
                 (jnp.sum(gate_grad * gate_grad, axis=0), jnp.sum(val_grad * val_grad, axis=0))
-            )
+            ),
         )
 
         placed = [own_rows]

time: 279 us -> 236 us (0.85)
  local copies, waits for them, and re-layouts: 65.8 us -> 13.6 us
  Pallas kernels: 24.1 us -> 42.4 us
  matrix products: 26.1 us -> 15.4 us
  other arithmetic: 15.3 us -> 9.18 us
  waiting for transfers between devices: 102 us -> 108 us
  starting transfers between devices: 42.4 us -> 45.3 us
    dynamic_slice x3 -> x0, local copies, waits for them, and re-layouts: 23 us -> none  [side(): return lax.dynamic_slice_in_dim(part, core, 1, axis=1)[:, 0]]
    pallas_call x0 -> x2, Pallas kernels: none -> 18.4 us  [partial_rows(): pl.pallas_call(functools.partial(rows_kernel, len(backs), fa, chips, core...]
    unnamed x63 -> x36, local copies, waits for them, and re-layouts: 17.4 us -> 3.09 us
    dot_general x20 -> x16, matrix products: 26.1 us -> 15.4 us  [dot(): lax.dot_general(left, right, dims, preferred_element_type=jnp.float32)]
    ppermute x7, waiting for transfers between devices: 25.2 us -> 33.2 us  [from_b(): return lax.ppermute(values, 'fs', perm)]
    reshape x2 -> x0, local copies, waits for them, and re-layouts: 7.68 us -> none  [reduced(): part = jnp.concatenate([dot(back, weight, over_hidden).astype(jnp.bfloat1...]
    dynamic_update_slice x10, local copies, waits for them, and re-layouts: 9.82 us -> 2.54 us  [local(): whole = lax.dynamic_update_slice(whole, held[dist, d][None], (place, 0, 0))]
    squeeze x2 -> x4, local copies, waits for them, and re-layouts: 0.13 us -> 3.68 us  [the longest x2 3.58 us: reduced(): other = from_core(part[1])]
  transfers between devices with their start and end apart: 33 -> 34, of which waited for: 16 -> 17; matrix products, arithmetic and copies ran while one was open for 36% -> 13% of each run, Pallas kernels for 0% -> 8%
where the time goes in v1:
time: 236 us; the launch traced here: 235 us
  waiting for transfers between devices  108 us (46%)
  starting transfers between devices  45.3 us (19%)
  Pallas kernels  42.4 us (18%)
  matrix products  15.4 us (7%)
  local copies, waits for them, and re-layouts  13.6 us (6%)
  other arithmetic  9.18 us (4%)
    ppermute x15, waiting for transfers between devices, from_chip(): return lax.ppermute(values, 'tp', perm)  50.2 us
    ppermute x7, waiting for transfers between devices, from_b(): return lax.ppermute(values, 'fs', perm)  33.2 us
    ppermute x15, starting transfers between devices, from_chip(): return lax.ppermute(values, 'tp', perm)  28.3 us
    pallas_call x4, Pallas kernels, chunk_backs(): pl.pallas_call(functools.partial(backs_kernel, group), grid=(1,), in_spec...  24 us
    ppermute x7, waiting for transfers between devices, from_a(): return lax.ppermute(values, 'fs', perm)  23 us
    pallas_call x2, Pallas kernels, partial_rows(): pl.pallas_call(functools.partial(rows_kernel, len(backs), fa, chips, core...  18.4 us
    dot_general x16, matrix products, dot(): lax.dot_general(left, right, dims, preferred_element_type=jnp.float32)  15.4 us
    ppermute x7, starting transfers between devices, from_b(): return lax.ppermute(values, 'fs', perm)  8.32 us
  transfers between devices with their start and end apart: 34, of which 17 were waited for; matrix products, arithmetic and copies ran while one was open for 13% of the time, Pallas kernels for 8%

profile of v1, /device:TPU:0, one launch (start us, length us, event | category | flops | bytes accessed | tf_op | source)
XLA Modules:
  0.0 235.2 jit_solution(12149593698221114816)
XLA Ops:
  2.3 5.9 %shard_map.143 = (bf16[352,1024]{1,0:T(8,128)(2,1)}, f32[176,6]{1,0:T(8,128)}) custom-call(bf16[704,1024]{1,0:T(8,128)(2,1)} %bitcast.144, bf16[704,1024]{1,0:T(8,128)(2,1)} %bitcast.148, bf16[704,1024]{1,0:T(8,128)(2,1)} %bitcast.152, f32[704,6]{1,0:T(8,128)} %bitcast.164), custom_call_target="tpu_custom_call" | custom-call | flops 10813440 | bytes 1802240 | tf_op jit(solution)/shard_map/pallas_call | solution.py:72
  8.2 6.0 %shard_map.144 = (bf16[352,1024]{1,0:T(8,128)(2,1)}, f32[176,6]{1,0:T(8,128)}) custom-call(bf16[704,1024]{1,0:T(8,128)(2,1)} %bitcast.145, bf16[704,1024]{1,0:T(8,128)(2,1)} %bitcast.149, bf16[704,1024]{1,0:T(8,128)(2,1)} %bitcast.153, f32[704,6]{1,0:T(8,128)} %bitcast.165), custom_call_target="tpu_custom_call" | custom-call | flops 10813440 | bytes 1802240 | tf_op jit(solution)/shard_map/pallas_call | solution.py:72
  14.2 6.0 %shard_map.145 = (bf16[352,1024]{1,0:T(8,128)(2,1)}, f32[176,6]{1,0:T(8,128)}) custom-call(bf16[704,1024]{1,0:T(8,128)(2,1)} %bitcast.146, bf16[704,1024]{1,0:T(8,128)(2,1)} %bitcast.150, bf16[704,1024]{1,0:T(8,128)(2,1)} %bitcast.154, f32[704,6]{1,0:T(8,128)} %bitcast.166), custom_call_target="tpu_custom_call" | custom-call | flops 10813440 | bytes 1802240 | tf_op jit(solution)/shard_map/pallas_call | solution.py:72
  20.2 6.1 %shard_map.146 = (bf16[352,1024]{1,0:T(8,128)(2,1)}, f32[176,6]{1,0:T(8,128)}) custom-call(bf16[704,1024]{1,0:T(8,128)(2,1)} %bitcast.147, bf16[704,1024]{1,0:T(8,128)(2,1)} %bitcast.151, bf16[704,1024]{1,0:T(8,128)(2,1)} %bitcast.155, f32[704,6]{1,0:T(8,128)} %bitcast.167), custom_call_target="tpu_custom_call" | custom-call | flops 10813440 | bytes 1802240 | tf_op jit(solution)/shard_map/pallas_call | solution.py:72
  27.7 3.0 %collective-permute-start.24 = (f32[6,704]{1,0:T(8,128)S(1)}, f32[6,704]{1,0:T(8,128)S(1)}, u32[]{:S(2)}, u32[]{:S(2)}) collective-permute-start(f32[6,704]{1,0:T(8,128)S(1)} %maximum_bitcast_fusion.1), channel_id=1, source_target_pairs={{8,0},{0,8},{24,16},{16,24},{9,1},{1,9},{25,17},{17,25},{10,2},{2,... | collective-permute-start | bytes 50696 | tf_op jit(solution)/shard_map/ppermute | solution.py:154
  40.2 3.6 %collective-permute-start.31 = (f32[2,3]{1,0:T(2,128)S(1)}, f32[2,3]{1,0:T(2,128)S(1)}, u32[]{:S(2)}, u32[]{:S(2)}) collective-permute-start(f32[2,3]{1,0:T(2,128)S(1)} %add.353), channel_id=1, source_target_pairs={{2,0},{3,1},{4,2},{5,3},{6,4},{7,5},{0,6},{1,7},{10,8},{11,9},{12,... | collective-permute-start | bytes 80 | tf_op jit(solution)/shard_map/ppermute | solution.py:168
  46.3 3.2 %collective-permute-done.32 = f32[2,3]{1,0:T(2,128)S(1)} collective-permute-done((f32[2,3]{1,0:T(2,128)S(1)}, f32[2,3]{1,0:T(2,128)S(1)}, u32[]{:S(2)}, u32[]{:S(2)}) %collective-permute-start.32) | collective-permute-done | bytes 56 | tf_op jit(solution)/shard_map/ppermute | solution.py:168
  51.3 3.9 %collective-permute-done.33 = f32[2,3]{1,0:T(2,128)S(1)} collective-permute-done((f32[2,3]{1,0:T(2,128)S(1)}, f32[2,3]{1,0:T(2,128)S(1)}, u32[]{:S(2)}, u32[]{:S(2)}) %collective-permute-start.33) | collective-permute-done | bytes 56 | tf_op jit(solution)/shard_map/ppermute | solution.py:168
  60.8 10.0 %collective-permute-done.7.refs_1_ = bf16[352,1024]{1,0:T(8,128)(2,1)} collective-permute-done((bf16[352,1024]{1,0:T(8,128)(2,1)}, bf16[352,1024]{1,0:T(8,128)(2,1)}, u32[]{:S(2)}, u32[]{:S(2)}) %collective-permute-start.7) | collective-permute-done | bytes 720928 | tf_op jit(solution)/shard_map/ppermute | solution.py:154
  70.8 3.6 %collective-permute-start.16 = (bf16[2,128,1024]{2,1,0:T(8,128)(2,1)}, bf16[2,128,1024]{2,1,0:T(8,128)(2,1)}, u32[]{:S(2)}, u32[]{:S(2)}) collective-permute-start(bf16[2,128,1024]{2,1,0:T(8,128)(2,1)} %get-tuple-element.64), channel_id=1, source_target_pairs={{2,0},{3,1},{4,2},{5,3},{6,4},{7,5},{0,6},{1,7},{10,8},{11,9},{12,... | collective-permute-start | bytes 1572872 | tf_op jit(solution)/shard_map/ppermute | solution.py:168
  74.4 11.7 %collective-permute-done.8.refs_2_ = bf16[352,1024]{1,0:T(8,128)(2,1)S(1)} collective-permute-done((bf16[352,1024]{1,0:T(8,128)(2,1)}, bf16[352,1024]{1,0:T(8,128)(2,1)S(1)}, u32[]{:S(2)}, u32[]{:S(2)}) %collective-permute-start.8) | collective-permute-done | bytes 720928 | tf_op jit(solution)/shard_map/ppermute | solution.py:154
  86.2 2.6 %collective-permute-start.17 = (bf16[2,128,1024]{2,1,0:T(8,128)(2,1)}, bf16[2,128,1024]{2,1,0:T(8,128)(2,1)}, u32[]{:S(2)}, u32[]{:S(2)}) collective-permute-start(bf16[2,128,1024]{2,1,0:T(8,128)(2,1)} %get-tuple-element.64), channel_id=1, source_target_pairs={{4,0},{5,1},{6,2},{7,3},{0,4},{1,5},{2,6},{3,7},{12,8},{13,9},{14,... | collective-permute-start | bytes 1572872 | tf_op jit(solution)/shard_map/ppermute | solution.py:168
  88.8 11.4 %collective-permute-done.9.refs_3_ = bf16[352,1024]{1,0:T(8,128)(2,1)S(1)} collective-permute-done((bf16[352,1024]{1,0:T(8,128)(2,1)}, bf16[352,1024]{1,0:T(8,128)(2,1)S(1)}, u32[]{:S(2)}, u32[]{:S(2)}) %collective-permute-start.9) | collective-permute-done | bytes 720928 | tf_op jit(solution)/shard_map/ppermute | solution.py:154
  102.9 9.2 %shard_map.148 = bf16[2,4,128,1024]{3,2,1,0:T(8,128)(2,1)} custom-call(s32[2]{0:T(128)} %pad_add_fusion.at_ref, bf16[352,1024]{1,0:T(8,128)(2,1)} %copy-done.4, bf16[352,1024]{1,0:T(8,128)(2,1)} %collective-permute-done.7.refs_1_, bf16[352,1024]{1,0:T(8,128)(2,1)} %copy-done.6, bf16[352,1024]{1,0:T(8,128)(2,1)} %copy-done.8, ...), custom_call_target="tpu_custom_call" | custom-call | flops 2952790016 | bytes 7864320 | tf_op jit(solution)/shard_map/pallas_call | solution.py:130
  114.4 9.2 %shard_map.147 = bf16[2,4,128,1024]{3,2,1,0:T(8,128)(2,1)} custom-call(s32[2]{0:T(128)} %pad_add_fusion.at_ref, bf16[352,1024]{1,0:T(8,128)(2,1)} %get-tuple-element.16.refs_0_, bf16[352,1024]{1,0:T(8,128)(2,1)} %get-tuple-element.17.refs_1_, bf16[352,1024]{1,0:T(8,128)(2,1)} %get-tuple-element.18.refs_2_, bf16[352,1024]{1,0:T(8,128)(2,1)} %get-tuple-element.19.refs_3_, ...), custom_call_target="tpu_custom_call" | custom-call | flops 2952790016 | bytes 7864320 | tf_op jit(solution)/shard_map/pallas_call | solution.py:130
  136.7 2.3 collective-permute-start.3
  143.3 15.7 %collective-permute-done.12 = bf16[128,1024]{1,0:T(8,128)(2,1)S(1)} collective-permute-done((bf16[128,1024]{1,0:T(8,128)(2,1)S(1)}, bf16[128,1024]{1,0:T(8,128)(2,1)S(1)}, u32[]{:S(2)}, u32[]{:S(2)}) %collective-permute-start.12) | collective-permute-done | bytes 262176 | tf_op jit(solution)/shard_map/ppermute | solution.py:168
  159.9 20.4 %collective-permute-done.4 = bf16[128,1024]{1,0:T(8,128)(2,1)S(1)} collective-permute-done((bf16[128,1024]{1,0:T(8,128)(2,1)S(1)}, bf16[128,1024]{1,0:T(8,128)(2,1)S(1)}, u32[]{:S(2)}, u32[]{:S(2)}) %collective-permute-start.4) | collective-permute-done | bytes 262176 | tf_op jit(solution)/shard_map/ppermute | solution.py:168
  198.4 2.6 %collective-permute-done.20 = bf16[352,512]{1,0:T(8,128)(2,1)S(1)} collective-permute-done((bf16[352,512]{1,0:T(8,128)(2,1)S(1)}, bf16[352,512]{1,0:T(8,128)(2,1)S(1)}, u32[]{:S(2)}, u32[]{:S(2)}) %collective-permute-start.20) | collective-permute-done | bytes 360480 | tf_op jit(solution)/shard_map/ppermute | solution.py:160
  201.6 7.1 %collective-permute-done.21 = bf16[352,512]{1,0:T(8,128)(2,1)S(1)} collective-permute-done((bf16[352,512]{1,0:T(8,128)(2,1)S(1)}, bf16[352,512]{1,0:T(8,128)(2,1)S(1)}, u32[]{:S(2)}, u32[]{:S(2)}) %collective-permute-start.21) | collective-permute-done | bytes 360480 | tf_op jit(solution)/shard_map/ppermute | solution.py:160
  210.4 6.1 %collective-permute-done.22 = bf16[352,512]{1,0:T(8,128)(2,1)S(1)} collective-permute-done((bf16[352,512]{1,0:T(8,128)(2,1)S(1)}, bf16[352,512]{1,0:T(8,128)(2,1)S(1)}, u32[]{:S(2)}, u32[]{:S(2)}) %collective-permute-start.22) | collective-permute-done | bytes 360480 | tf_op jit(solution)/shard_map/ppermute | solution.py:160
  217.1 5.5 %collective-permute-done.23 = bf16[352,512]{1,0:T(8,128)(2,1)S(1)} collective-permute-done((bf16[352,512]{1,0:T(8,128)(2,1)S(1)}, bf16[352,512]{1,0:T(8,128)(2,1)S(1)}, u32[]{:S(2)}, u32[]{:S(2)}) %collective-permute-start.23) | collective-permute-done | bytes 360480 | tf_op jit(solution)/shard_map/ppermute | solution.py:160
  226.5 2.7 %collective-permute-start.28 = (f32[2,512]{1,0:T(2,128)S(1)}, f32[2,512]{1,0:T(2,128)S(1)}, u32[]{:S(2)}, u32[]{:S(2)}) collective-permute-start(f32[2,512]{1,0:T(2,128)S(1)} %fusion.58), channel_id=1, source_target_pairs={{4,0},{5,1},{6,2},{7,3},{0,4},{1,5},{2,6},{3,7},{12,8},{13,9},{14,... | collective-permute-start | bytes 12296 | tf_op jit(solution)/shard_map/ppermute | solution.py:168
  231.2 3.4 %collective-permute-done.29 = f32[2,512]{1,0:T(2,128)S(1)} collective-permute-done((f32[2,512]{1,0:T(2,128)S(1)}, f32[2,512]{1,0:T(2,128)S(1)}, u32[]{:S(2)}, u32[]{:S(2)}) %collective-permute-start.29) | collective-permute-done | bytes 4128 | tf_op jit(solution)/shard_map/ppermute | solution.py:168
  (155 shorter events, 72.7 us)
Async XLA Ops:
  30.7 26.6 %collective-permute-start.6 = (bf16[352,1024]{1,0:T(8,128)(2,1)S(1)}, bf16[352,1024]{1,0:T(8,128)(2,1)S(1)}, u32[]{:S(2)}, u32[]{:S(2)}) collective-permute-start(bf16[352,1024]{1,0:T(8,128)(2,1)S(1)} %copy-done.15), channel_id=1, source_target_pairs={{8,0},{0,8},{24,16},{16,24},{9,1},{1,9},{25,17},{17,25},{10,2},{2,... | collective-permute-start | bytes 2162696 | tf_op jit(solution)/shard_map/ppermute | solution.py:154
  30.8 24.9 %collective-permute-start.15 = (bf16[128,1024]{1,0:T(8,128)(2,1)S(1)}, bf16[128,1024]{1,0:T(8,128)(2,1)S(1)}, u32[]{:S(2)}, u32[]{:S(2)}) collective-permute-start(bf16[128,1024]{1,0:T(8,128)(2,1)S(1)} %pad_maximum_fusion.4), channel_id=1, source_target_pairs={{8,0},{0,8},{24,16},{16,24},{9,1},{1,9},{25,17},{17,25},{10,2},{2,... | collective-permute-start | bytes 786440 | tf_op jit(solution)/shard_map/ppermute | solution.py:154
  32.8 38.0 %collective-permute-start.7 = (bf16[352,1024]{1,0:T(8,128)(2,1)}, bf16[352,1024]{1,0:T(8,128)(2,1)}, u32[]{:S(2)}, u32[]{:S(2)}) collective-permute-start(bf16[352,1024]{1,0:T(8,128)(2,1)} %get-tuple-element.17.refs_1_), channel_id=1, source_target_pairs={{8,0},{0,8},{24,16},{16,24},{9,1},{1,9},{25,17},{17,25},{10,2},{2,... | collective-permute-start | bytes 2162696 | tf_op jit(solution)/shard_map/ppermute | solution.py:154
  32.9 53.3 %collective-permute-start.8 = (bf16[352,1024]{1,0:T(8,128)(2,1)}, bf16[352,1024]{1,0:T(8,128)(2,1)S(1)}, u32[]{:S(2)}, u32[]{:S(2)}) collective-permute-start(bf16[352,1024]{1,0:T(8,128)(2,1)} %get-tuple-element.18.refs_2_), channel_id=1, source_target_pairs={{8,0},{0,8},{24,16},{16,24},{9,1},{1,9},{25,17},{17,25},{10,2},{2,... | collective-permute-start | bytes 2162696 | tf_op jit(solution)/shard_map/ppermute | solution.py:154
  55.2 45.0 %collective-permute-start.9 = (bf16[352,1024]{1,0:T(8,128)(2,1)}, bf16[352,1024]{1,0:T(8,128)(2,1)S(1)}, u32[]{:S(2)}, u32[]{:S(2)}) collective-permute-start(bf16[352,1024]{1,0:T(8,128)(2,1)} %get-tuple-element.19.refs_3_), channel_id=1, source_target_pairs={{8,0},{0,8},{24,16},{16,24},{9,1},{1,9},{25,17},{17,25},{10,2},{2,... | collective-permute-start | bytes 2162696 | tf_op jit(solution)/shard_map/ppermute | solution.py:154
  55.7 47.2 %collective-permute-start = (bf16[704,512]{1,0:T(8,128)(2,1)}, bf16[704,512]{1,0:T(8,128)(2,1)}, u32[]{:S(2)}, u32[]{:S(2)}) collective-permute-start(bf16[704,512]{1,0:T(8,128)(2,1)} %bitcast.6.refs_4_), channel_id=1, source_target_pairs={{16,0},{24,8},{0,16},{8,24},{17,1},{25,9},{1,17},{9,25},{18,2},{26... | collective-permute-start | bytes 2162696 | tf_op jit(solution)/shard_map/ppermute | solution.py:160
  57.2 45.7 %collective-permute-start.1 = (bf16[704,512]{1,0:T(8,128)(2,1)}, bf16[704,512]{1,0:T(8,128)(2,1)}, u32[]{:S(2)}, u32[]{:S(2)}) collective-permute-start(bf16[704,512]{1,0:T(8,128)(2,1)} %bitcast.7.refs_6_), channel_id=1, source_target_pairs={{16,0},{24,8},{0,16},{8,24},{17,1},{25,9},{1,17},{9,25},{18,2},{26... | collective-permute-start | bytes 2162696 | tf_op jit(solution)/shard_map/ppermute | solution.py:160
  70.8 54.6 %collective-permute-start.16 = (bf16[2,128,1024]{2,1,0:T(8,128)(2,1)}, bf16[2,128,1024]{2,1,0:T(8,128)(2,1)}, u32[]{:S(2)}, u32[]{:S(2)}) collective-permute-start(bf16[2,128,1024]{2,1,0:T(8,128)(2,1)} %get-tuple-element.64), channel_id=1, source_target_pairs={{2,0},{3,1},{4,2},{5,3},{6,4},{7,5},{0,6},{1,7},{10,8},{11,9},{12,... | collective-permute-start | bytes 1572872 | tf_op jit(solution)/shard_map/ppermute | solution.py:168
  86.2 39.3 %collective-permute-start.17 = (bf16[2,128,1024]{2,1,0:T(8,128)(2,1)}, bf16[2,128,1024]{2,1,0:T(8,128)(2,1)}, u32[]{:S(2)}, u32[]{:S(2)}) collective-permute-start(bf16[2,128,1024]{2,1,0:T(8,128)(2,1)} %get-tuple-element.64), channel_id=1, source_target_pairs={{4,0},{5,1},{6,2},{7,3},{0,4},{1,5},{2,6},{3,7},{12,8},{13,9},{14,... | collective-permute-start | bytes 1572872 | tf_op jit(solution)/shard_map/ppermute | solution.py:168
  101.1 24.3 %collective-permute-start.18 = (bf16[2,128,1024]{2,1,0:T(8,128)(2,1)}, bf16[2,128,1024]{2,1,0:T(8,128)(2,1)S(1)}, u32[]{:S(2)}, u32[]{:S(2)}) collective-permute-start(bf16[2,128,1024]{2,1,0:T(8,128)(2,1)} %get-tuple-element.64), channel_id=1, source_target_pairs={{6,0},{7,1},{0,2},{1,3},{2,4},{3,5},{4,6},{5,7},{14,8},{15,9},{8,1... | collective-permute-start | bytes 1572872 | tf_op jit(solution)/shard_map/ppermute | solution.py:168
  114.4 15.3 %collective-permute-start.10 = (bf16[4,128,1024]{2,1,0:T(8,128)(2,1)}, bf16[4,128,1024]{2,1,0:T(8,128)(2,1)}, u32[]{:S(2)}, u32[]{:S(2)}) collective-permute-start(bf16[4,128,1024]{2,1,0:T(8,128)(2,1)} %slice_bitcast_fusion), channel_id=1, source_target_pairs={{1,0},{0,1},{3,2},{2,3},{5,4},{4,5},{7,6},{6,7},{9,8},{8,9},{11,10... | collective-permute-start | bytes 3145736 | tf_op jit(solution)/shard_map/ppermute | solution.py:172
  124.9 11.3 %collective-permute-start.2 = (bf16[4,128,1024]{2,1,0:T(8,128)(2,1)S(1)}, bf16[4,128,1024]{2,1,0:T(8,128)(2,1)S(1)}, u32[]{:S(2)}, u32[]{:S(2)}) collective-permute-start(bf16[4,128,1024]{2,1,0:T(8,128)(2,1)S(1)} %slice_bitcast_fusion.2), channel_id=1, source_target_pairs={{1,0},{0,1},{3,2},{2,3},{5,4},{4,5},{7,6},{6,7},{9,8},{8,9},{11,10... | collective-permute-start | bytes 3145736 | tf_op jit(solution)/shard_map/ppermute | solution.py:172
  127.1 53.5 %collective-permute-start.19 = (bf16[4,2,128,1024]{3,2,1,0:T(8,128)(2,1)S(1)}, bf16[4,2,128,1024]{3,2,1,0:T(8,128)(2,1)S(1)}, u32[]{:S(2)}, u32[]{:S(2)}) collective-permute-start(bf16[4,2,128,1024]{3,2,1,0:T(8,128)(2,1)S(1)} %pad_maximum_fusion), channel_id=1, source_target_pairs={{1,0},{0,1},{3,2},{2,3},{5,4},{4,5},{7,6},{6,7},{9,8},{8,9},{11,10... | collective-permute-start | bytes 6291464 | tf_op jit(solution)/shard_map/ppermute | solution.py:172
  131.5 9.7 %collective-permute-start.11 = (bf16[128,1024]{1,0:T(8,128)(2,1)S(1)}, bf16[128,1024]{1,0:T(8,128)(2,1)S(1)}, u32[]{:S(2)}, u32[]{:S(2)}) collective-permute-start(bf16[128,1024]{1,0:T(8,128)(2,1)S(1)} %get-tuple-element.44), channel_id=1, source_target_pairs={{2,0},{3,1},{4,2},{5,3},{6,4},{7,5},{0,6},{1,7},{10,8},{11,9},{12,... | collective-permute-start | bytes 786440 | tf_op jit(solution)/shard_map/ppermute | solution.py:168
  133.6 25.4 %collective-permute-start.12 = (bf16[128,1024]{1,0:T(8,128)(2,1)S(1)}, bf16[128,1024]{1,0:T(8,128)(2,1)S(1)}, u32[]{:S(2)}, u32[]{:S(2)}) collective-permute-start(bf16[128,1024]{1,0:T(8,128)(2,1)S(1)} %get-tuple-element.46), channel_id=1, source_target_pairs={{4,0},{5,1},{6,2},{7,3},{0,4},{1,5},{2,6},{3,7},{12,8},{13,9},{14,... | collective-permute-start | bytes 786440 | tf_op jit(solution)/shard_map/ppermute | solution.py:168
  134.6 24.5 %collective-permute-start.13 = (bf16[128,1024]{1,0:T(8,128)(2,1)S(1)}, bf16[128,1024]{1,0:T(8,128)(2,1)S(1)}, u32[]{:S(2)}, u32[]{:S(2)}) collective-permute-start(bf16[128,1024]{1,0:T(8,128)(2,1)S(1)} %get-tuple-element.45), channel_id=1, source_target_pairs={{6,0},{7,1},{0,2},{1,3},{2,4},{3,5},{4,6},{5,7},{14,8},{15,9},{8,1... | collective-permute-start | bytes 786440 | tf_op jit(solution)/shard_map/ppermute | solution.py:168
  136.7 23.3 %collective-permute-start.3 = (bf16[128,1024]{1,0:T(8,128)(2,1)S(1)}, bf16[128,1024]{1,0:T(8,128)(2,1)S(1)}, u32[]{:S(2)}, u32[]{:S(2)}) collective-permute-start(bf16[128,1024]{1,0:T(8,128)(2,1)S(1)} %get-tuple-element.47), channel_id=1, source_target_pairs={{2,0},{3,1},{4,2},{5,3},{6,4},{7,5},{0,6},{1,7},{10,8},{11,9},{12,... | collective-permute-start | bytes 786440 | tf_op jit(solution)/shard_map/ppermute | solution.py:168
  141.2 39.2 %collective-permute-start.4 = (bf16[128,1024]{1,0:T(8,128)(2,1)S(1)}, bf16[128,1024]{1,0:T(8,128)(2,1)S(1)}, u32[]{:S(2)}, u32[]{:S(2)}) collective-permute-start(bf16[128,1024]{1,0:T(8,128)(2,1)S(1)} %get-tuple-element.49), channel_id=1, source_target_pairs={{4,0},{5,1},{6,2},{7,3},{0,4},{1,5},{2,6},{3,7},{12,8},{13,9},{14,... | collective-permute-start | bytes 786440 | tf_op jit(solution)/shard_map/ppermute | solution.py:168
  159.0 21.3 %collective-permute-start.5 = (bf16[128,1024]{1,0:T(8,128)(2,1)S(1)}, bf16[128,1024]{1,0:T(8,128)(2,1)S(1)}, u32[]{:S(2)}, u32[]{:S(2)}) collective-permute-start(bf16[128,1024]{1,0:T(8,128)(2,1)S(1)} %get-tuple-element.48), channel_id=1, source_target_pairs={{6,0},{7,1},{0,2},{1,3},{2,4},{3,5},{4,6},{5,7},{14,8},{15,9},{8,1... | collective-permute-start | bytes 786440 | tf_op jit(solution)/shard_map/ppermute | solution.py:168
  159.3 66.0 %collective-permute-start.14 = (bf16[128,1024]{1,0:T(8,128)(2,1)S(1)}, bf16[128,1024]{1,0:T(8,128)(2,1)S(1)}, u32[]{:S(2)}, u32[]{:S(2)}) collective-permute-start(bf16[128,1024]{1,0:T(8,128)(2,1)S(1)} %fusion.38), channel_id=1, source_target_pairs={{8,0},{0,8},{24,16},{16,24},{9,1},{1,9},{25,17},{17,25},{10,2},{2,... | collective-permute-start | bytes 786440 | tf_op jit(solution)/shard_map/ppermute | solution.py:154
  189.6 11.4 %collective-permute-start.20 = (bf16[352,512]{1,0:T(8,128)(2,1)S(1)}, bf16[352,512]{1,0:T(8,128)(2,1)S(1)}, u32[]{:S(2)}, u32[]{:S(2)}) collective-permute-start(bf16[352,512]{1,0:T(8,128)(2,1)S(1)} %fusion.6), channel_id=1, source_target_pairs={{16,0},{24,8},{0,16},{8,24},{17,1},{25,9},{1,17},{9,25},{18,2},{26... | collective-permute-start | bytes 1081352 | tf_op jit(solution)/shard_map/ppermute | solution.py:160
  192.9 15.8 %collective-permute-start.21 = (bf16[352,512]{1,0:T(8,128)(2,1)S(1)}, bf16[352,512]{1,0:T(8,128)(2,1)S(1)}, u32[]{:S(2)}, u32[]{:S(2)}) collective-permute-start(bf16[352,512]{1,0:T(8,128)(2,1)S(1)} %fusion.7), channel_id=1, source_target_pairs={{16,0},{24,8},{0,16},{8,24},{17,1},{25,9},{1,17},{9,25},{18,2},{26... | collective-permute-start | bytes 1081352 | tf_op jit(solution)/shard_map/ppermute | solution.py:160
  194.0 22.4 %collective-permute-start.22 = (bf16[352,512]{1,0:T(8,128)(2,1)S(1)}, bf16[352,512]{1,0:T(8,128)(2,1)S(1)}, u32[]{:S(2)}, u32[]{:S(2)}) collective-permute-start(bf16[352,512]{1,0:T(8,128)(2,1)S(1)} %fusion.8), channel_id=1, source_target_pairs={{16,0},{24,8},{0,16},{8,24},{17,1},{25,9},{1,17},{9,25},{18,2},{26... | collective-permute-start | bytes 1081352 | tf_op jit(solution)/shard_map/ppermute | solution.py:160
  196.1 26.4 %collective-permute-start.23 = (bf16[352,512]{1,0:T(8,128)(2,1)S(1)}, bf16[352,512]{1,0:T(8,128)(2,1)S(1)}, u32[]{:S(2)}, u32[]{:S(2)}) collective-permute-start(bf16[352,512]{1,0:T(8,128)(2,1)S(1)} %fusion.9), channel_id=1, source_target_pairs={{16,0},{24,8},{0,16},{8,24},{17,1},{25,9},{1,17},{9,25},{18,2},{26... | collective-permute-start | bytes 1081352 | tf_op jit(solution)/shard_map/ppermute | solution.py:160
  (28 other events, 118.5 us)
